TPU v7x, 32 devices: a whole 2x2x4 slice. The times are simulated.
32 devices in a mesh: grp: 2 (over x), sp: 4 (over y, core), tp: 4 (over z).
Axes of the slice: x: 2, y: 2, z: 4, core: 2. Of those that a mesh axis runs over, the one named last changes fastest.
Arguments:
- tokens_in: bfloat16 [2048, 2048], P(('grp', 'sp'), 'tp'), parts along dimension 0, may hold values from -8 to 8
- out_gate: bfloat16 [3, 2048, 2048], P(None, 'sp', 'tp'), may hold values from -0.125 to 0.125
- in_gate: bfloat16 [3, 2048, 2048], P(None, 'sp', 'tp'), may hold values from -0.125 to 0.125
- value_proj: bfloat16 [3, 2048, 2048], P(None, 'sp', 'tp'), may hold values from -0.125 to 0.125
- mix_proj: bfloat16 [3, 2048, 2048], P(None, 'sp', 'tp'), may hold values from -0.125 to 0.125
- conv_taps: float32 [3, 3, 2048], P(None, None, 'tp'), may hold values from -3.5 to 3.5
- norm_gains: float32 [3, 2048], P(None, 'tp'), may hold values from 0.1 to 1.9
- final_gain: float32 [2048], P('tp'), may hold values from 0.1 to 1.9
Outputs:
- normed_out: bfloat16 [2048, 2048], P(('grp', 'sp'), 'tp'), parts along dimension 0
There are 2 independent parts, one for each index of `grp`. A program takes and returns all parts, laid end to end along the dimension named above; an argument that names none is the same for every part. Nothing has to cross between parts.
All inputs are finite; a program needn't handle non-finite values.
Results may differ from a plain program's by a relative error of at most 0.025.
Values may be sent and summed in bfloat16 or wider, within the bound.
A program may use at most 64 MiB of HBM per device.

v0:
```python
import jax
import jax.numpy as jnp
from jax import lax
from jax.sharding import PartitionSpec as P

D = 2048
TAPS = 3
LAYERS = 3
epsilon = 1e-06


def passed_along(shard, axis, by):
    peers = lax.axis_size(axis)
    pairs = [(i, i + by) for i in range(peers) if 0 <= i + by < peers]
    return lax.ppermute(shard, axis, pairs)


def row_scale(stream):
    squares = lax.psum(jnp.sum(stream * stream, axis=1, keepdims=True), "tp")
    return lax.rsqrt(squares / D + epsilon)


def shards(tokens_in, out_gate, in_gate, value_proj, mix_proj, conv_taps, norm_gains, final_gain):
    stream = tokens_in.astype(jnp.float32)
    row_count = stream.shape[0]
    reach = TAPS - 1
    whole = (
        lax.all_gather(out_gate, "sp", axis=1, tiled=True),
        lax.all_gather(in_gate, "sp", axis=1, tiled=True),
        lax.all_gather(value_proj, "sp", axis=1, tiled=True),
        lax.all_gather(mix_proj, "sp", axis=1, tiled=True),
    )
    for layer_index in range(LAYERS):
        scale = row_scale(stream)
        normed = (stream * norm_gains[layer_index]).astype(jnp.bfloat16)
        gathered = lax.all_gather(normed, "tp", axis=1, tiled=True)
        products = tuple(
            (
                jnp.dot(gathered, weight[layer_index], preferred_element_type=jnp.float32)
                for weight in whole[:3]
            )
        )
        out_gates, in_gates, values = [
            (product * scale).astype(jnp.bfloat16) for product in products
        ]
        product_v = (in_gates.astype(jnp.float32) * values.astype(jnp.float32)).astype(jnp.bfloat16)
        earlier = passed_along(product_v[row_count - reach :], "sp", 1)
        padded = jnp.concatenate([earlier, product_v], axis=0)
        convolved = padded[0:row_count].astype(jnp.float32) * conv_taps[layer_index, 0]
        for tap_index in range(1, TAPS):
            convolved = (
                convolved
                + padded[tap_index : tap_index + row_count].astype(jnp.float32)
                * conv_taps[layer_index, tap_index]
            )
        gated = (out_gates.astype(jnp.float32) * convolved).astype(jnp.bfloat16)
        spread = lax.all_gather(gated, "tp", axis=1, tiled=True)
        mixed = jnp.dot(spread, whole[3][layer_index], preferred_element_type=jnp.float32)
        stream = stream + mixed
    scale = row_scale(stream)
    return (stream * scale * final_gain).astype(jnp.bfloat16)


def solution(mesh):
    in_specs = (
        P(("grp", "sp"), "tp"),
        P(None, "sp", "tp"),
        P(None, "sp", "tp"),
        P(None, "sp", "tp"),
        P(None, "sp", "tp"),
        P(None, None, "tp"),
        P(None, "tp"),
        P("tp"),
    )
    out_specs = P(("grp", "sp"), "tp")
    return jax.shard_map(shards, mesh=mesh, in_specs=in_specs, out_specs=out_specs, check_vma=False)
```

profile of v0, /device:TPU:0, one launch (start us, length us, event | category | flops | bytes accessed | tf_op | source)
XLA Modules:
  0.0 424.5 jit_solution(9574232206159354128)
XLA Ops:
  6.5 0.8 fusion.60
  7.4 1.7 fusion.55
  11.8 13.5 %psum.28 = f32[256,1]{0,1:T(1,128)S(1)} all-reduce(f32[256,1]{0,1:T(1,128)S(1)} %bitcast.159), channel_id=1, replica_groups=mesh['grp'=2,'sp'=4,'tp'=4] {'tp'}, use_global_device_ids=true, to_apply=%region_1.0 | all-reduce | flops 256 | bytes 2048 | tf_op jit(solution)/shard_map/psum | solution.py:19
  25.3 14.7 %all-gather.11.cloned.1.call-done = bf16[256,2048]{1,0:T(8,128)(2,1)} async-done(((bf16[256,512]{1,0:T(8,128)(2,1)}), bf16[256,2048]{1,0:T(8,128)(2,1)}) %all-gather.11.cloned.1.call-update) | async-done | bytes 1048592 | tf_op jit(solution)/shard_map/all_gather | solution.py:36
  40.0 47.3 %all-gather.17.cloned.1.call-done = bf16[3,2048,512]{2,1,0:T(8,128)(2,1)} async-done(((bf16[3,512,512]{2,1,0:T(8,128)(2,1)}), bf16[3,2048,512]{2,1,0:T(8,128)(2,1)}) %all-gather.17.cloned.1.call-update) | async-done | bytes 6291472 | tf_op jit(solution)/shard_map/all_gather | solution.py:30
  87.3 2.6 fusion.39
  90.0 45.3 %all-gather.15.cloned.1.call-done = bf16[3,2048,512]{2,1,0:T(8,128)(2,1)} async-done(((bf16[3,512,512]{2,1,0:T(8,128)(2,1)}), bf16[3,2048,512]{2,1,0:T(8,128)(2,1)}) %all-gather.15.cloned.1.call-update) | async-done | bytes 6291472 | tf_op jit(solution)/shard_map/all_gather | solution.py:29
  135.3 2.6 fusion.38
  137.9 2.2 collective-permute-start
  140.1 43.0 %all-gather.13.cloned.1.call-done = bf16[3,2048,512]{2,1,0:T(8,128)(2,1)} async-done(((bf16[3,512,512]{2,1,0:T(8,128)(2,1)}), bf16[3,2048,512]{2,1,0:T(8,128)(2,1)}) %all-gather.13.cloned.1.call-update) | async-done | bytes 6291472 | tf_op jit(solution)/shard_map/all_gather | solution.py:28
  183.1 3.1 fusion.35
  186.3 44.6 %all-gather.21.cloned.1.call-done = bf16[3,2048,512]{2,1,0:T(8,128)(2,1)} async-done(((bf16[3,512,512]{2,1,0:T(8,128)(2,1)}), bf16[3,2048,512]{2,1,0:T(8,128)(2,1)}) %all-gather.21.cloned.1.call-update) | async-done | bytes 6291472 | tf_op jit(solution)/shard_map/all_gather | solution.py:31
  230.9 29.4 %all-gather.19.cloned.1.call-done = bf16[256,2048]{1,0:T(8,128)(2,1)} async-done(((bf16[256,512]{1,0:T(8,128)(2,1)}), bf16[256,2048]{1,0:T(8,128)(2,1)}) %all-gather.19.cloned.1.call-update) | async-done | bytes 1048592 | tf_op jit(solution)/shard_map/all_gather | solution.py:57
  260.3 3.4 multiply_reduce_fusion.2
  263.8 10.3 %psum.29 = f32[256,1]{0,1:T(1,128)S(1)} all-reduce(f32[256,1]{0,1:T(1,128)S(1)} %bitcast.182), channel_id=1, replica_groups=mesh['grp'=2,'sp'=4,'tp'=4] {'tp'}, use_global_device_ids=true, to_apply=%region_3.0 | all-reduce | flops 256 | bytes 2048 | tf_op jit(solution)/shard_map/psum | solution.py:19
  274.1 17.2 %all-gather.23.cloned.1.call-done = bf16[256,2048]{1,0:T(8,128)(2,1)} async-done(((bf16[256,512]{1,0:T(8,128)(2,1)}), bf16[256,2048]{1,0:T(8,128)(2,1)}) %all-gather.23.cloned.1.call-update) | async-done | bytes 1048592 | tf_op jit(solution)/shard_map/all_gather | solution.py:36
  291.2 2.7 fusion.46
  293.9 2.6 fusion.45
  296.6 1.3 collective-permute-start.1
  298.7 3.1 fusion.42
  301.9 30.3 %all-gather.25.cloned.1.call-done = bf16[256,2048]{1,0:T(8,128)(2,1)} async-done(((bf16[256,512]{1,0:T(8,128)(2,1)}), bf16[256,2048]{1,0:T(8,128)(2,1)}) %all-gather.25.cloned.1.call-update) | async-done | bytes 1048592 | tf_op jit(solution)/shard_map/all_gather | solution.py:57
  332.2 3.3 multiply_reduce_fusion.1
  335.6 10.3 %psum.30 = f32[256,1]{0,1:T(1,128)S(1)} all-reduce(f32[256,1]{0,1:T(1,128)S(1)} %bitcast.181), channel_id=1, replica_groups=mesh['grp'=2,'sp'=4,'tp'=4] {'tp'}, use_global_device_ids=true, to_apply=%region_5.0 | all-reduce | flops 256 | bytes 2048 | tf_op jit(solution)/shard_map/psum | solution.py:19
  345.9 17.2 %all-gather.27.cloned.1.call-done = bf16[256,2048]{1,0:T(8,128)(2,1)} async-done(((bf16[256,512]{1,0:T(8,128)(2,1)}), bf16[256,2048]{1,0:T(8,128)(2,1)}) %all-gather.27.cloned.1.call-update) | async-done | bytes 1048592 | tf_op jit(solution)/shard_map/all_gather | solution.py:36
  363.0 2.7 fusion.53
  365.7 2.6 fusion.52
  368.4 1.3 collective-permute-start.2
  370.5 3.1 fusion.49
  373.6 30.3 %all-gather.29.cloned.1.call-done = bf16[256,2048]{1,0:T(8,128)(2,1)} async-done(((bf16[256,512]{1,0:T(8,128)(2,1)}), bf16[256,2048]{1,0:T(8,128)(2,1)}) %all-gather.29.cloned.1.call-update) | async-done | bytes 1048592 | tf_op jit(solution)/shard_map/all_gather | solution.py:57
  404.0 2.7 multiply_reduce_fusion
  406.7 10.2 %psum.31 = f32[256,1]{0,1:T(1,128)S(1)} all-reduce(f32[256,1]{0,1:T(1,128)S(1)} %bitcast.183), channel_id=1, replica_groups=mesh['grp'=2,'sp'=4,'tp'=4] {'tp'}, use_global_device_ids=true, to_apply=%region_7.0 | all-reduce | flops 256 | bytes 2048 | tf_op jit(solution)/shard_map/psum | solution.py:19
  416.8 0.8 multiply_convert_fusion
  (43 shorter events, 4.6 us)
Async XLA Ops:
  6.5 33.5 %all-gather.11.cloned.1.call-start = ((), (), s32[]{:S(2)}) async-start(), calls=%async_computation | async-start | bytes 1310720 | tf_op jit(solution)/shard_map/all_gather | solution.py:36
  9.1 78.2 %all-gather.17.cloned.1.call-start = ((), (), s32[]{:S(2)}) async-start(), calls=%async_computation.3 | async-start | bytes 7864320 | tf_op jit(solution)/shard_map/all_gather | solution.py:30
  9.9 125.4 %all-gather.15.cloned.1.call-start = ((), (), s32[]{:S(2)}) async-start(), calls=%async_computation.2 | async-start | bytes 7864320 | tf_op jit(solution)/shard_map/all_gather | solution.py:29
  10.6 129.5 %copy-start.1 = (f32[3,3,512]{2,1,0:T(4,128)S(1)}, f32[3,3,512]{2,1,0:T(4,128)}, u32[]{:S(2)}) copy-start(f32[3,3,512]{2,1,0:T(4,128)} %param.13) | copy-start | bytes 55300
  10.6 172.5 %all-gather.13.cloned.1.call-start = ((), (), s32[]{:S(2)}) async-start(), calls=%async_computation.1 | async-start | bytes 7864320 | tf_op jit(solution)/shard_map/all_gather | solution.py:28
  11.2 219.7 %all-gather.21.cloned.1.call-start = ((), (), s32[]{:S(2)}) async-start(), calls=%async_computation.5 | async-start | bytes 7864320 | tf_op jit(solution)/shard_map/all_gather | solution.py:31
  11.8 248.6 %all-gather.19.cloned.1.call-start = ((), (), s32[]{:S(2)}) async-start(), calls=%async_computation.4 | async-start | bytes 1310720 | tf_op jit(solution)/shard_map/all_gather | solution.py:57
  40.0 143.1 %copy-start.3 = (bf16[256,2048]{1,0:T(8,128)(2,1)S(1)}, bf16[256,2048]{1,0:T(8,128)(2,1)}, u32[]{:S(2)}) copy-start(bf16[256,2048]{1,0:T(8,128)(2,1)} %all-gather.11.cloned.1.call-done) | copy-start | bytes 3145732
  90.0 170.4 %copy-start = (bf16[256,512]{1,0:T(8,128)(2,1)S(1)}, bf16[256,512]{1,0:T(8,128)(2,1)}, u32[]{:S(2)}) copy-start(bf16[256,512]{1,0:T(8,128)(2,1)} %param.8) | copy-start | bytes 786436
  137.9 45.2 %collective-permute-start = (bf16[2,512]{1,0:T(2,128)(2,1)S(1)}, bf16[2,512]{1,0:T(2,128)(2,1)S(1)}, u32[]{:S(2)}, u32[]{:S(2)}) collective-permute-start(bf16[2,512]{1,0:T(2,128)(2,1)S(1)} %slice.135), channel_id=1, source_target_pairs={{0,4},{4,8},{8,12},{1,5},{5,9},{9,13},{2,6},{6,10},{10,14},{3,7},{... | collective-permute-start | bytes 6152 | tf_op jit(solution)/shard_map/ppermute | solution.py:15
  186.2 105.0 %all-gather.23.cloned.1.call-start = ((), (), s32[]{:S(2)}) async-start(), calls=%async_computation.6 | async-start | bytes 1310720 | tf_op jit(solution)/shard_map/all_gather | solution.py:36
  263.7 68.4 %all-gather.25.cloned.1.call-start = ((), (), s32[]{:S(2)}) async-start(), calls=%async_computation.7 | async-start | bytes 1310720 | tf_op jit(solution)/shard_map/all_gather | solution.py:57
  291.2 7.5 %copy-start.5 = (bf16[256,2048]{1,0:T(8,128)(2,1)S(1)}, bf16[256,2048]{1,0:T(8,128)(2,1)}, u32[]{:S(2)}) copy-start(bf16[256,2048]{1,0:T(8,128)(2,1)} %all-gather.23.cloned.1.call-done) | copy-start | bytes 3145732
  296.6 2.1 collective-permute-start.1
  301.8 61.2 %all-gather.27.cloned.1.call-start = ((), (), s32[]{:S(2)}) async-start(), calls=%async_computation.8 | async-start | bytes 1310720 | tf_op jit(solution)/shard_map/all_gather | solution.py:36
  335.5 68.4 %all-gather.29.cloned.1.call-start = ((), (), s32[]{:S(2)}) async-start(), calls=%async_computation.9 | async-start | bytes 1310720 | tf_op jit(solution)/shard_map/all_gather | solution.py:57
  363.0 7.5 %copy-start.4 = (bf16[256,2048]{1,0:T(8,128)(2,1)S(1)}, bf16[256,2048]{1,0:T(8,128)(2,1)}, u32[]{:S(2)}) copy-start(bf16[256,2048]{1,0:T(8,128)(2,1)} %all-gather.27.cloned.1.call-done) | copy-start | bytes 3145732
  368.4 48.5 %copy-start.2 = (f32[512]{0:T(512)S(1)}, f32[512]{0:T(512)}, u32[]{:S(2)}) copy-start(f32[512]{0:T(512)} %param.15) | copy-start | bytes 6148
  368.4 2.1 collective-permute-start.2
Sparse Core Ops, SparseCore 0:
  9.2 30.7 all-gather.10
  41.6 45.7 all-gather.16
  88.9 46.3 all-gather.14
  136.7 46.3 all-gather.12
  184.5 46.3 all-gather.20
  232.3 27.9 all-gather.18
  263.8 27.3 all-gather.22
  302.0 30.1 all-gather.24
  335.6 27.3 all-gather.26
  373.8 30.1 all-gather.28
where the time goes:
time: 425 us
  waiting for transfers between devices  323 us (76%)
  blocking collectives  44.2 us (10%)
  matrix products  34.6 us (8%)
  between operations  13.7 us (3%)
  starting transfers between devices  5.1 us (1%)
    all_gather x3, waiting for transfers between devices, shards(): spread = lax.all_gather(gated, 'tp', axis=1, tiled=True)  90 us
    all_gather x3, waiting for transfers between devices, shards(): gathered = lax.all_gather(normed, 'tp', axis=1, tiled=True)  49.1 us
    all_gather x1, waiting for transfers between devices, shards(): lax.all_gather(value_proj, 'sp', axis=1, tiled=True)  47.3 us
    all_gather x1, waiting for transfers between devices, shards(): lax.all_gather(in_gate, 'sp', axis=1, tiled=True)  45.3 us
    all_gather x1, waiting for transfers between devices, shards(): lax.all_gather(mix_proj, 'sp', axis=1, tiled=True)  44.6 us
    psum x4, blocking collectives, row_scale(): squares = lax.psum(jnp.sum(stream * stream, axis=1, keepdims=True), 'tp')  44.2 us
    all_gather x1, waiting for transfers between devices, shards(): lax.all_gather(out_gate, 'sp', axis=1, tiled=True)  43 us
    dot_general x9, matrix products, shards(): jnp.dot(gathered, weight[layer_index], preferred_element_type=jnp.float32)  25.2 us
  transfers between devices with their start and end apart: 13, of which 12 were waited for; matrix products, arithmetic and copies ran while one was open for 2% of the time, Pallas kernels for 0%

commit v1 on v0

--- a/solution.py
+++ b/solution.py
@@ -1,3 +1,4 @@
+import functools
 import jax
 import jax.numpy as jnp
 from jax import lax
@@ -7,6 +8,23 @@
 TAPS = 3
 LAYERS = 3
 epsilon = 1e-06
+
+
+def build_the_side(own_rows, mesh_ax, d0):
+    n = lax.axis_size(mesh_ax)
+    v1 = sorted(((dev, (dev + 1) % n) for dev in range(n)))
+    piece_now = own_rows
+    items = [piece_now]
+    for hop_no in range(1, n):
+        piece_now = lax.ppermute(piece_now, mesh_ax, v1)
+        items.insert(0, piece_now)
+    val = jnp.concatenate(items, axis=d0)
+    g_now = lax.axis_index(mesh_ax) + 1
+    formed = jnp.roll(val, shift=g_now * own_rows.shape[d0], axis=d0)
+    return formed
+
+
+_expand_task = functools.partial(build_the_side, mesh_ax="tp", d0=1)
 
 
 def passed_along(shard, axis, by):
@@ -33,7 +51,7 @@
     for layer_index in range(LAYERS):
         scale = row_scale(stream)
         normed = (stream * norm_gains[layer_index]).astype(jnp.bfloat16)
-        gathered = lax.all_gather(normed, "tp", axis=1, tiled=True)
+        gathered = _expand_task(normed)
         products = tuple(
             (
                 jnp.dot(gathered, weight[layer_index], preferred_element_type=jnp.float32)

time: 425 us -> 399 us (0.939)
  waiting for transfers between devices: 323 us -> 290 us
  starting transfers between devices: 5.1 us -> 11.1 us
    ppermute x0 -> x9, waiting for transfers between devices: none -> 50.4 us  [build_the_side(): piece_now = lax.ppermute(piece_now, mesh_ax, v1)]
    all_gather x3 -> x0, waiting for transfers between devices: 49.1 us -> none  [shards(): gathered = lax.all_gather(normed, 'tp', axis=1, tiled=True)]
    all_gather x1, waiting for transfers between devices: 47.3 us -> 14.2 us  [shards(): lax.all_gather(value_proj, 'sp', axis=1, tiled=True)]
    ppermute x0 -> x9, starting transfers between devices: none -> 6.11 us  [build_the_side(): piece_now = lax.ppermute(piece_now, mesh_ax, v1)]
  transfers between devices with their start and end apart: 13 -> 19, of which waited for: 12 -> 15; matrix products, arithmetic and copies ran while one was open for 2% -> 2% of each run, Pallas kernels for 0% -> 0%
where the time goes in v1:
time: 399 us; the launch traced here: 398 us
  waiting for transfers between devices  290 us (73%)
  blocking collectives  46.6 us (12%)
  matrix products  31.3 us (8%)
  between operations  13.7 us (3%)
  starting transfers between devices  11.1 us (3%)
  other arithmetic  5.01 us (1%)
    all_gather x3, waiting for transfers between devices, shards(): spread = lax.all_gather(gated, 'tp', axis=1, tiled=True)  87.6 us
    ppermute x9, waiting for transfers between devices, build_the_side(): piece_now = lax.ppermute(piece_now, mesh_ax, v1)  50.4 us
    psum x4, blocking collectives, row_scale(): squares = lax.psum(jnp.sum(stream * stream, axis=1, keepdims=True), 'tp')  46.6 us
    all_gather x1, waiting for transfers between devices, shards(): lax.all_gather(in_gate, 'sp', axis=1, tiled=True)  45.6 us
    all_gather x1, waiting for transfers between devices, shards(): lax.all_gather(mix_proj, 'sp', axis=1, tiled=True)  44.6 us
    all_gather x1, waiting for transfers between devices, shards(): lax.all_gather(out_gate, 'sp', axis=1, tiled=True)  43.4 us
    dot_general x9, matrix products, shards(): jnp.dot(gathered, weight[layer_index], preferred_element_type=jnp.float32)  23.1 us
    all_gather x1, waiting for transfers between devices, shards(): lax.all_gather(value_proj, 'sp', axis=1, tiled=True)  14.2 us
  transfers between devices with their start and end apart: 19, of which 15 were waited for; matrix products, arithmetic and copies ran while one was open for 2% of the time, Pallas kernels for 0%

profile of v1, /device:TPU:0, one launch (start us, length us, event | category | flops | bytes accessed | tf_op | source)
XLA Modules:
  0.0 397.9 jit_solution(16695529249188009231)
XLA Ops:
  9.6 3.1 collective-permute-start
  12.7 8.3 %collective-permute-done = bf16[256,512]{1,0:T(8,128)(2,1)S(1)} collective-permute-done((bf16[256,512]{1,0:T(8,128)(2,1)S(1)}, bf16[256,512]{1,0:T(8,128)(2,1)S(1)}, u32[]{:S(2)}, u32[]{:S(2)}) %collective-permute-start) | collective-permute-done | bytes 262176 | tf_op jit(solution)/shard_map/ppermute | solution.py:19
  21.0 9.3 %collective-permute-done.1 = bf16[256,512]{1,0:T(8,128)(2,1)S(1)} collective-permute-done((bf16[256,512]{1,0:T(8,128)(2,1)S(1)}, bf16[256,512]{1,0:T(8,128)(2,1)S(1)}, u32[]{:S(2)}, u32[]{:S(2)}) %collective-permute-start.1) | collective-permute-done | bytes 262176 | tf_op jit(solution)/shard_map/ppermute | solution.py:19
  30.3 12.2 %psum.28 = f32[256,1]{0,1:T(1,128)S(1)} all-reduce(f32[256,1]{0,1:T(1,128)S(1)} %bitcast.159), channel_id=1, replica_groups=mesh['grp'=2,'sp'=4,'tp'=4] {'tp'}, use_global_device_ids=true, to_apply=%region_1.3 | all-reduce | flops 256 | bytes 2048 | tf_op jit(solution)/shard_map/psum | solution.py:37
  43.8 14.2 %all-gather.12.cloned.1.call-done = bf16[3,2048,512]{2,1,0:T(8,128)(2,1)} async-done(((bf16[3,512,512]{2,1,0:T(8,128)(2,1)}), bf16[3,2048,512]{2,1,0:T(8,128)(2,1)}) %all-gather.12.cloned.1.call-update) | async-done | bytes 6291472 | tf_op jit(solution)/shard_map/all_gather | solution.py:48
  58.0 2.3 fusion.39
  60.3 45.6 %all-gather.10.cloned.1.call-done = bf16[3,2048,512]{2,1,0:T(8,128)(2,1)} async-done(((bf16[3,512,512]{2,1,0:T(8,128)(2,1)}), bf16[3,2048,512]{2,1,0:T(8,128)(2,1)}) %all-gather.10.cloned.1.call-update) | async-done | bytes 6291472 | tf_op jit(solution)/shard_map/all_gather | solution.py:47
  106.0 2.3 fusion.38
  108.3 2.2 collective-permute-start.3
  110.5 43.4 %all-gather.8.cloned.1.call-done = bf16[3,2048,512]{2,1,0:T(8,128)(2,1)} async-done(((bf16[3,512,512]{2,1,0:T(8,128)(2,1)}), bf16[3,2048,512]{2,1,0:T(8,128)(2,1)}) %all-gather.8.cloned.1.call-update) | async-done | bytes 6291472 | tf_op jit(solution)/shard_map/all_gather | solution.py:46
  153.9 3.1 fusion.35
  157.1 44.6 %all-gather.16.cloned.1.call-done = bf16[3,2048,512]{2,1,0:T(8,128)(2,1)} async-done(((bf16[3,512,512]{2,1,0:T(8,128)(2,1)}), bf16[3,2048,512]{2,1,0:T(8,128)(2,1)}) %all-gather.16.cloned.1.call-update) | async-done | bytes 6291472 | tf_op jit(solution)/shard_map/all_gather | solution.py:49
  201.7 29.4 %all-gather.14.cloned.1.call-done = bf16[256,2048]{1,0:T(8,128)(2,1)} async-done(((bf16[256,512]{1,0:T(8,128)(2,1)}), bf16[256,2048]{1,0:T(8,128)(2,1)}) %all-gather.14.cloned.1.call-update) | async-done | bytes 1048592 | tf_op jit(solution)/shard_map/all_gather | solution.py:75
  231.2 2.7 multiply_reduce_fusion.2
  233.9 1.5 collective-permute-start.4
  235.4 7.9 %collective-permute-done.4 = bf16[256,512]{1,0:T(8,128)(2,1)S(1)} collective-permute-done((bf16[256,512]{1,0:T(8,128)(2,1)S(1)}, bf16[256,512]{1,0:T(8,128)(2,1)S(1)}, u32[]{:S(2)}, u32[]{:S(2)}) %collective-permute-start.4) | collective-permute-done | bytes 262176 | tf_op jit(solution)/shard_map/ppermute | solution.py:19
  243.3 8.5 %collective-permute-done.5 = bf16[256,512]{1,0:T(8,128)(2,1)S(1)} collective-permute-done((bf16[256,512]{1,0:T(8,128)(2,1)S(1)}, bf16[256,512]{1,0:T(8,128)(2,1)S(1)}, u32[]{:S(2)}, u32[]{:S(2)}) %collective-permute-start.5) | collective-permute-done | bytes 262176 | tf_op jit(solution)/shard_map/ppermute | solution.py:19
  251.8 12.2 %psum.29 = f32[256,1]{0,1:T(1,128)S(1)} all-reduce(f32[256,1]{0,1:T(1,128)S(1)} %bitcast.182), channel_id=1, replica_groups=mesh['grp'=2,'sp'=4,'tp'=4] {'tp'}, use_global_device_ids=true, to_apply=%region_3.5 | all-reduce | flops 256 | bytes 2048 | tf_op jit(solution)/shard_map/psum | solution.py:37
  265.3 2.3 fusion.46
  267.6 2.3 fusion.45
  272.1 3.1 fusion.42
  275.3 29.0 %all-gather.18.cloned.1.call-done = bf16[256,2048]{1,0:T(8,128)(2,1)} async-done(((bf16[256,512]{1,0:T(8,128)(2,1)}), bf16[256,2048]{1,0:T(8,128)(2,1)}) %all-gather.18.cloned.1.call-update) | async-done | bytes 1048592 | tf_op jit(solution)/shard_map/all_gather | solution.py:75
  304.3 2.7 multiply_reduce_fusion.1
  308.5 7.9 %collective-permute-done.8 = bf16[256,512]{1,0:T(8,128)(2,1)S(1)} collective-permute-done((bf16[256,512]{1,0:T(8,128)(2,1)S(1)}, bf16[256,512]{1,0:T(8,128)(2,1)S(1)}, u32[]{:S(2)}, u32[]{:S(2)}) %collective-permute-start.8) | collective-permute-done | bytes 262176 | tf_op jit(solution)/shard_map/ppermute | solution.py:19
  316.5 8.5 %collective-permute-done.9 = bf16[256,512]{1,0:T(8,128)(2,1)S(1)} collective-permute-done((bf16[256,512]{1,0:T(8,128)(2,1)S(1)}, bf16[256,512]{1,0:T(8,128)(2,1)S(1)}, u32[]{:S(2)}, u32[]{:S(2)}) %collective-permute-start.9) | collective-permute-done | bytes 262176 | tf_op jit(solution)/shard_map/ppermute | solution.py:19
  325.0 12.2 %psum.30 = f32[256,1]{0,1:T(1,128)S(1)} all-reduce(f32[256,1]{0,1:T(1,128)S(1)} %bitcast.181), channel_id=1, replica_groups=mesh['grp'=2,'sp'=4,'tp'=4] {'tp'}, use_global_device_ids=true, to_apply=%region_5.7 | all-reduce | flops 256 | bytes 2048 | tf_op jit(solution)/shard_map/psum | solution.py:37
  338.5 2.3 fusion.53
  340.8 2.3 fusion.52
  345.2 3.1 fusion.49
  348.3 29.1 %all-gather.20.cloned.1.call-done = bf16[256,2048]{1,0:T(8,128)(2,1)} async-done(((bf16[256,512]{1,0:T(8,128)(2,1)}), bf16[256,2048]{1,0:T(8,128)(2,1)}) %all-gather.20.cloned.1.call-update) | async-done | bytes 1048592 | tf_op jit(solution)/shard_map/all_gather | solution.py:75
  377.4 2.7 multiply_reduce_fusion
  380.1 10.2 %psum.31 = f32[256,1]{0,1:T(1,128)S(1)} all-reduce(f32[256,1]{0,1:T(1,128)S(1)} %bitcast.183), channel_id=1, replica_groups=mesh['grp'=2,'sp'=4,'tp'=4] {'tp'}, use_global_device_ids=true, to_apply=%region_7.9 | all-reduce | flops 256 | bytes 2048 | tf_op jit(solution)/shard_map/psum | solution.py:37
  (51 shorter events, 13.7 us)
Async XLA Ops:
  6.5 51.5 %all-gather.12.cloned.1.call-start = ((), (), s32[]{:S(2)}) async-start(), calls=%async_computation.2 | async-start | bytes 7864320 | tf_op jit(solution)/shard_map/all_gather | solution.py:48
  7.3 2.1 copy-start.2
  7.3 2.1 copy-start
  7.3 98.7 %all-gather.10.cloned.1.call-start = ((), (), s32[]{:S(2)}) async-start(), calls=%async_computation.1 | async-start | bytes 7864320 | tf_op jit(solution)/shard_map/all_gather | solution.py:47
  8.0 145.9 %all-gather.8.cloned.1.call-start = ((), (), s32[]{:S(2)}) async-start(), calls=%async_computation | async-start | bytes 7864320 | tf_op jit(solution)/shard_map/all_gather | solution.py:46
  8.8 193.0 %all-gather.16.cloned.1.call-start = ((), (), s32[]{:S(2)}) async-start(), calls=%async_computation.4 | async-start | bytes 7864320 | tf_op jit(solution)/shard_map/all_gather | solution.py:49
  9.3 221.8 %all-gather.14.cloned.1.call-start = ((), (), s32[]{:S(2)}) async-start(), calls=%async_computation.3 | async-start | bytes 1310720 | tf_op jit(solution)/shard_map/all_gather | solution.py:75
  9.6 11.4 %collective-permute-start = (bf16[256,512]{1,0:T(8,128)(2,1)S(1)}, bf16[256,512]{1,0:T(8,128)(2,1)S(1)}, u32[]{:S(2)}, u32[]{:S(2)}) collective-permute-start(bf16[256,512]{1,0:T(8,128)(2,1)S(1)} %get-tuple-element.11), channel_id=1, source_target_pairs={{0,1},{1,2},{2,3},{3,0},{4,5},{5,6},{6,7},{7,4},{8,9},{9,10},{10,1... | collective-permute-start | bytes 786440 | tf_op jit(solution)/shard_map/ppermute | solution.py:19
  21.0 9.3 %collective-permute-start.1 = (bf16[256,512]{1,0:T(8,128)(2,1)S(1)}, bf16[256,512]{1,0:T(8,128)(2,1)S(1)}, u32[]{:S(2)}, u32[]{:S(2)}) collective-permute-start(bf16[256,512]{1,0:T(8,128)(2,1)S(1)} %collective-permute-done), channel_id=1, source_target_pairs={{0,1},{1,2},{2,3},{3,0},{4,5},{5,6},{6,7},{7,4},{8,9},{9,10},{10,1... | collective-permute-start | bytes 786440 | tf_op jit(solution)/shard_map/ppermute | solution.py:19
  30.3 12.2 %collective-permute-start.2 = (bf16[256,512]{1,0:T(8,128)(2,1)S(1)}, bf16[256,512]{1,0:T(8,128)(2,1)S(1)}, u32[]{:S(2)}, u32[]{:S(2)}) collective-permute-start(bf16[256,512]{1,0:T(8,128)(2,1)S(1)} %collective-permute-done.1), channel_id=1, source_target_pairs={{0,1},{1,2},{2,3},{3,0},{4,5},{5,6},{6,7},{7,4},{8,9},{9,10},{10,1... | collective-permute-start | bytes 786440 | tf_op jit(solution)/shard_map/ppermute | solution.py:19
  60.3 50.1 %copy-start.1 = (f32[3,3,512]{2,1,0:T(4,128)S(1)}, f32[3,3,512]{2,1,0:T(4,128)}, u32[]{:S(2)}) copy-start(f32[3,3,512]{2,1,0:T(4,128)} %param.15) | copy-start | bytes 55300
  108.3 45.6 %collective-permute-start.3 = (bf16[2,512]{1,0:T(2,128)(2,1)S(1)}, bf16[2,512]{1,0:T(2,128)(2,1)S(1)}, u32[]{:S(2)}, u32[]{:S(2)}) collective-permute-start(bf16[2,512]{1,0:T(2,128)(2,1)S(1)} %slice.135), channel_id=1, source_target_pairs={{0,4},{4,8},{8,12},{1,5},{5,9},{9,13},{2,6},{6,10},{10,14},{3,7},{... | collective-permute-start | bytes 6152 | tf_op jit(solution)/shard_map/ppermute | solution.py:33
  157.0 147.3 %all-gather.18.cloned.1.call-start = ((), (), s32[]{:S(2)}) async-start(), calls=%async_computation.5 | async-start | bytes 1310720 | tf_op jit(solution)/shard_map/all_gather | solution.py:75
  233.9 9.4 %collective-permute-start.4 = (bf16[256,512]{1,0:T(8,128)(2,1)S(1)}, bf16[256,512]{1,0:T(8,128)(2,1)S(1)}, u32[]{:S(2)}, u32[]{:S(2)}) collective-permute-start(bf16[256,512]{1,0:T(8,128)(2,1)S(1)} %get-tuple-element.9), channel_id=1, source_target_pairs={{0,1},{1,2},{2,3},{3,0},{4,5},{5,6},{6,7},{7,4},{8,9},{9,10},{10,1... | collective-permute-start | bytes 786440 | tf_op jit(solution)/shard_map/ppermute | solution.py:19
  243.3 8.5 %collective-permute-start.5 = (bf16[256,512]{1,0:T(8,128)(2,1)S(1)}, bf16[256,512]{1,0:T(8,128)(2,1)S(1)}, u32[]{:S(2)}, u32[]{:S(2)}) collective-permute-start(bf16[256,512]{1,0:T(8,128)(2,1)S(1)} %collective-permute-done.4), channel_id=1, source_target_pairs={{0,1},{1,2},{2,3},{3,0},{4,5},{5,6},{6,7},{7,4},{8,9},{9,10},{10,1... | collective-permute-start | bytes 786440 | tf_op jit(solution)/shard_map/ppermute | solution.py:19
  251.8 12.2 %collective-permute-start.6 = (bf16[256,512]{1,0:T(8,128)(2,1)S(1)}, bf16[256,512]{1,0:T(8,128)(2,1)S(1)}, u32[]{:S(2)}, u32[]{:S(2)}) collective-permute-start(bf16[256,512]{1,0:T(8,128)(2,1)S(1)} %collective-permute-done.5), channel_id=1, source_target_pairs={{0,1},{1,2},{2,3},{3,0},{4,5},{5,6},{6,7},{7,4},{8,9},{9,10},{10,1... | collective-permute-start | bytes 786440 | tf_op jit(solution)/shard_map/ppermute | solution.py:19
  270.0 2.1 collective-permute-start.7
  275.2 102.2 %all-gather.20.cloned.1.call-start = ((), (), s32[]{:S(2)}) async-start(), calls=%async_computation.6 | async-start | bytes 1310720 | tf_op jit(solution)/shard_map/all_gather | solution.py:75
  307.0 9.4 %collective-permute-start.8 = (bf16[256,512]{1,0:T(8,128)(2,1)S(1)}, bf16[256,512]{1,0:T(8,128)(2,1)S(1)}, u32[]{:S(2)}, u32[]{:S(2)}) collective-permute-start(bf16[256,512]{1,0:T(8,128)(2,1)S(1)} %get-tuple-element.7), channel_id=1, source_target_pairs={{0,1},{1,2},{2,3},{3,0},{4,5},{5,6},{6,7},{7,4},{8,9},{9,10},{10,1... | collective-permute-start | bytes 786440 | tf_op jit(solution)/shard_map/ppermute | solution.py:19
  316.5 8.5 %collective-permute-start.9 = (bf16[256,512]{1,0:T(8,128)(2,1)S(1)}, bf16[256,512]{1,0:T(8,128)(2,1)S(1)}, u32[]{:S(2)}, u32[]{:S(2)}) collective-permute-start(bf16[256,512]{1,0:T(8,128)(2,1)S(1)} %collective-permute-done.8), channel_id=1, source_target_pairs={{0,1},{1,2},{2,3},{3,0},{4,5},{5,6},{6,7},{7,4},{8,9},{9,10},{10,1... | collective-permute-start | bytes 786440 | tf_op jit(solution)/shard_map/ppermute | solution.py:19
  325.0 12.2 %collective-permute-start.10 = (bf16[256,512]{1,0:T(8,128)(2,1)S(1)}, bf16[256,512]{1,0:T(8,128)(2,1)S(1)}, u32[]{:S(2)}, u32[]{:S(2)}) collective-permute-start(bf16[256,512]{1,0:T(8,128)(2,1)S(1)} %collective-permute-done.9), channel_id=1, source_target_pairs={{0,1},{1,2},{2,3},{3,0},{4,5},{5,6},{6,7},{7,4},{8,9},{9,10},{10,1... | collective-permute-start | bytes 786440 | tf_op jit(solution)/shard_map/ppermute | solution.py:19
  343.1 2.1 collective-permute-start.11
  377.4 12.9 %copy-start.3 = (f32[512]{0:T(512)S(1)}, f32[512]{0:T(512)}, u32[]{:S(2)}) copy-start(f32[512]{0:T(512)} %param.17) | copy-start | bytes 6148
Sparse Core Ops, SparseCore 0:
  8.9 49.0 all-gather.11
  59.6 46.3 all-gather.9
  107.5 46.3 all-gather.7
  155.3 46.3 all-gather.15
  203.1 27.9 all-gather.13
  275.3 28.9 all-gather.17
  348.4 28.9 all-gather.19
